TPU v7x, 128 devices: a whole 4x4x4 slice. The times are simulated.
128 devices in a mesh: sp: 32 (over y, x, core), tp: 4 (over z).
Axes of the slice: x: 4, y: 4, z: 4, core: 2. Of those that a mesh axis runs over, the one named last changes fastest.
Arguments:
- block_input: bfloat16 [4096, 1024], P('sp'), may hold values from -6 to 6
- w_query: bfloat16 [1024, 1024], P(None, 'tp'), may hold values from -0.1875 to 0.1875
- w_forget_fwd: bfloat16 [1024, 1024], P(None, 'tp'), may hold values from -0.1875 to 0.1875
- w_forget_bwd: bfloat16 [1024, 1024], P(None, 'tp'), may hold values from -0.1875 to 0.1875
- w_value: bfloat16 [1024, 1024], P(None, 'tp'), may hold values from -0.1875 to 0.1875
- floor_rate: float32 [2, 1024], P(None, 'tp'), may hold values from 0.2 to 6
- gain: float32 [128], replicated, may hold values from 0.1 to 1.9
- cotangent: bfloat16 [4096, 1024], P('sp', 'tp'), may hold values from -6 to 6
Outputs:
- grad_input: bfloat16 [4096, 1024], P(('sp', 'tp'))
- grad_query_weight: float32 [1024, 1024], P('sp', 'tp')
- grad_floor: float32 [2, 1024], P(None, 'tp')
All inputs are finite; a program needn't handle non-finite values.
Results may differ from a plain program's by a relative error of at most 0.0045.
Values sent between devices are 32-bit elements.
A program may use at most 64 MiB of HBM per device.

v0:
```python
from functools import partial

import jax
import jax.numpy as jnp
from jax import lax
from jax.sharding import Mesh
from jax.sharding import PartitionSpec as P

KDIM = 128
SP = ("sp_0", "sp_1", "sp_2")
SP_TP = ("sp_0", "sp_1", "sp_2", "tp")


FINEST_ROUNDING = lax.Precision.HIGHEST
NORM_EPS = 1e-06


def neutral_like(array, identity):
    return jax.tree.map(
        lambda part, zero: jnp.zeros_like(part) + jnp.asarray(zero, part.dtype), array, identity
    )


def entering(array, axes, combine, identity, reverse):
    before = start = neutral_like(array, identity)
    subtotal = array
    for axis in reversed(axes):
        length, position = lax.axis_size(axis), lax.axis_index(axis)
        pieces = jax.tree.map(lambda part: lax.all_gather(part, axis), subtotal)
        inside, subtotal = start, start
        for k in reversed(range(length)) if reverse else range(length):
            passed = k > position if reverse else k < position
            subtotal = combine(subtotal, jax.tree.map(lambda part: part[k], pieces))
            inside = jax.tree.map(lambda new, old: jnp.where(passed, new, old), subtotal, inside)
        before = combine(inside, before)
    return before


def summed_rows(contribution, width, axis):
    whole = contribution(jnp.int32(0), width * lax.axis_size(axis))
    return lax.psum_scatter(whole, axis, scatter_dimension=0, tiled=True)


def one_axis_at_a_time(array, axes):
    for axis in axes:
        array = lax.psum(array, axis)
    return array


def gate_maps(raw_gate, floor_rates, seq_total):
    step_rate = floor_rates / seq_total
    opening = -jnp.expm1(-step_rate)
    log_forget = jnp.logaddexp(-step_rate, jnp.log(opening) + jax.nn.log_sigmoid(raw_gate))
    return (opening * jax.nn.sigmoid(-raw_gate), log_forget)


def span_output(queries, key_gate, log_forget, payload_entries, arriving_signal):
    cumul = jnp.cumsum(log_forget, axis=0)
    faded_asking_vector = queries * jnp.exp(cumul)
    k_dec = key_gate * jnp.exp(-cumul)
    tok_count = queries.shape[0]
    scores = jnp.einsum("thk,shk->hts", faded_asking_vector, k_dec, precision=FINEST_ROUNDING)
    scores = scores * jnp.tril(jnp.ones((tok_count, tok_count), jnp.float32))
    inner_part = jnp.einsum("hts,shv->thv", scores, payload_entries, precision=FINEST_ROUNDING)
    external_portion = jnp.einsum(
        "nea,eaw->new", faded_asking_vector, arriving_signal, precision=FINEST_ROUNDING
    )
    return inner_part + external_portion


def span_carry(key_gate, log_forget, payload_entries):
    cumul = jnp.cumsum(log_forget, axis=0)
    final_running_total = cumul[-1]
    scaled_by_factor = key_gate * jnp.exp(final_running_total[None] - cumul)
    return (
        jnp.exp(final_running_total),
        jnp.einsum("xzp,xzo->zpo", scaled_by_factor, payload_entries, precision=FINEST_ROUNDING),
    )


def span_exit(key_gate, log_forget, payload_entries, arriving_signal):
    keep_all, local_sum = span_carry(key_gate, log_forget, payload_entries)
    return keep_all[..., None] * arriving_signal + local_sum


def compose(earlier, later):
    return (earlier[0] * later[0], later[0][..., None] * earlier[1] + later[1])


def normed(mixed, gain):
    mean_square = jnp.mean(mixed * mixed, axis=-1, keepdims=True)
    return mixed * lax.rsqrt(mean_square + NORM_EPS) * gain


def body(block_input, w_query, w_forget_fwd, w_forget_bwd, w_value, floor_rate, gain, cotangent):
    tok_rows, in_width = block_input.shape
    head_count = w_query.shape[1] // KDIM
    val_dim = w_value.shape[1] // head_count
    seq_total = tok_rows * lax.axis_size(SP)
    q_scale = KDIM ** (-0.5)
    norm_scale = seq_total ** (-0.5)

    def project(weight, per_head):
        pre = jnp.dot(block_input, weight, preferred_element_type=jnp.float32).astype(jnp.bfloat16)
        return (
            lax.optimization_barrier(pre)
            .astype(jnp.float32)
            .reshape(tok_rows, head_count, per_head)
        )

    queries = project(w_query, KDIM) * q_scale
    payload_entries = project(w_value, val_dim)
    raw_fwd = project(w_forget_fwd, KDIM)
    raw_bwd = project(w_forget_bwd, KDIM)
    floor_rates = floor_rate.reshape(2, head_count, KDIM)

    def gate_both(gate_fwd, gate_bwd, rate_pair):
        return gate_maps(gate_fwd, rate_pair[0], float(seq_total)) + gate_maps(
            gate_bwd, rate_pair[1], float(seq_total)
        )

    gate_vals, gate_back = jax.vjp(gate_both, raw_fwd, raw_bwd, floor_rates)
    key_fwd, logf_fwd, key_bwd, logf_bwd = gate_vals
    flipped = partial(jnp.flip, axis=0)
    rev_query = flipped(queries)
    rev_key = flipped(key_bwd)
    rev_logf = flipped(logf_bwd)
    rev_value = flipped(payload_entries)
    identity = (
        jnp.ones((head_count, KDIM), jnp.float32),
        jnp.zeros((head_count, KDIM, val_dim), jnp.float32),
    )
    carry_fwd = span_carry(key_fwd, logf_fwd, payload_entries)
    carry_bwd = span_carry(rev_key, rev_logf, rev_value)
    inflow_fwd = entering(carry_fwd, SP, compose, identity, False)[1]
    inflow_bwd = entering(carry_bwd, SP, compose, identity, True)[1]
    mixed_fwd, back_fwd = jax.vjp(
        span_output, queries, key_fwd, logf_fwd, payload_entries, inflow_fwd
    )
    mixed_bwd, back_bwd = jax.vjp(span_output, rev_query, rev_key, rev_logf, rev_value, inflow_bwd)
    mixed = mixed_fwd + flipped(mixed_bwd)
    _, norm_back = jax.vjp(partial(normed, gain=gain), mixed)
    (d_mixed,) = norm_back(cotangent.astype(jnp.float32).reshape(tok_rows, head_count, val_dim))
    dq_fwd, dk_fwd, dlf_fwd, dv_fwd, seed_fwd = back_fwd(d_mixed)
    dq_bwd, dk_bwd, dlf_bwd, dv_bwd, seed_bwd = back_bwd(flipped(d_mixed))
    grad_q = ((dq_fwd + flipped(dq_bwd)) * q_scale).reshape(tok_rows, -1).astype(jnp.bfloat16)
    w_rows = in_width // lax.axis_size(SP)

    def weight_term(first_row, row_count):
        columns = lax.dynamic_slice_in_dim(block_input, first_row, row_count, 1)
        return lax.dot_general(
            columns, grad_q, (((0,), (0,)), ((), ())), preferred_element_type=jnp.float32
        )

    weight_sum = summed_rows(weight_term, w_rows, SP)
    outflow_fwd = entering((carry_fwd[0], seed_fwd), SP, compose, identity, True)[1]
    outflow_bwd = entering((carry_bwd[0], seed_bwd), SP, compose, identity, False)[1]
    _, exit_fwd = jax.vjp(span_exit, key_fwd, logf_fwd, payload_entries, inflow_fwd)
    _, exit_bwd = jax.vjp(span_exit, rev_key, rev_logf, rev_value, inflow_bwd)
    ek_fwd, elf_fwd, ev_fwd, _ = exit_fwd(outflow_fwd)
    ek_bwd, elf_bwd, ev_bwd, _ = exit_bwd(outflow_bwd)
    d_values = dv_fwd + ev_fwd + flipped(dv_bwd + ev_bwd)
    d_raw_fwd, d_raw_bwd, d_rates = gate_back(
        (dk_fwd + ek_fwd, dlf_fwd + elf_fwd, flipped(dk_bwd + ek_bwd), flipped(dlf_bwd + elf_bwd))
    )
    grad_weight = weight_sum * norm_scale
    grad_parts = (
        grad_q,
        d_raw_fwd.reshape(tok_rows, -1).astype(jnp.bfloat16),
        d_raw_bwd.reshape(tok_rows, -1).astype(jnp.bfloat16),
        d_values.reshape(tok_rows, -1).astype(jnp.bfloat16),
    )
    weight_parts = (w_query, w_forget_fwd, w_forget_bwd, w_value)

    def input_term(first_row, row_count):
        summed = jnp.zeros((row_count, in_width), jnp.float32)
        for grad_part, weight in zip(grad_parts, weight_parts):
            rows_part = lax.dynamic_slice_in_dim(grad_part, first_row, row_count, 0)
            summed = summed + lax.dot_general(
                rows_part, weight, (((1,), (1,)), ((), ())), preferred_element_type=jnp.float32
            )
        return summed

    grad_input = summed_rows(input_term, tok_rows // lax.axis_size("tp"), "tp").astype(jnp.bfloat16)
    grad_floor = one_axis_at_a_time(d_rates.reshape(2, -1), SP) * norm_scale
    return (grad_input, grad_weight, grad_floor)


def solution(mesh):
    finer = Mesh(mesh.devices.reshape(4, 4, 2, mesh.shape["tp"]), ("sp_0", "sp_1", "sp_2", "tp"))
    return jax.shard_map(
        body,
        mesh=finer,
        in_specs=(
            P(SP, None),
            P(None, "tp"),
            P(None, "tp"),
            P(None, "tp"),
            P(None, "tp"),
            P(None, "tp"),
            P(),
            P(SP, "tp"),
        ),
        out_specs=(P(SP_TP, None), P(SP, "tp"), P(None, "tp")),
        check_vma=False,
    )
```

profile of v0, /device:TPU:0, one launch (start us, length us, event | category | flops | bytes accessed | tf_op | source)
XLA Modules:
  0.0 358.0 jit_solution(10930753792484951539)
XLA Ops:
  9.1 1.4 convolution_convert_fusion.1
  11.8 1.3 broadcast_multiply_fusion.1
  14.7 1.8 all_gather.103
  17.1 9.9 %all_gather.104 = f32[4,2,128]{2,1,0:T(2,128)S(1)} all-gather(f32[1,2,128]{2,1,0:T(2,128)S(1)} %get-tuple-element.137), channel_id=1, replica_groups=mesh['sp_0'=4,'sp_1'=4,'sp_2'=2,'tp'=4] {'sp_1'}, dimensions={0}, use_global_device_ids=true | all-gather | bytes 5120 | tf_op jit(solution)/shard_map/all_gather | solution.py:29
  27.6 1.8 all_gather.96
  29.9 7.0 %all_gather.97 = f32[4,2,128]{2,1,0:T(2,128)S(1)} all-gather(f32[1,2,128]{2,1,0:T(2,128)S(1)} %get-tuple-element.142), channel_id=1, replica_groups=mesh['sp_0'=4,'sp_1'=4,'sp_2'=2,'tp'=4] {'sp_1'}, dimensions={0}, use_global_device_ids=true | all-gather | bytes 5120 | tf_op jit(solution)/shard_map/all_gather | solution.py:29
  44.3 2.0 all-gather.1
  46.4 12.8 %all_gather.108 = f32[4,2,128,128]{3,2,1,0:T(8,128)S(1)} all-gather(f32[1,2,128,128]{3,2,1,0:T(8,128)S(1)} %bitcast_add_fusion.16), channel_id=1, replica_groups=mesh['sp_0'=4,'sp_1'=4,'sp_2'=2,'tp'=4] {'sp_1'}, dimensions={0}, use_global_device_ids=true | all-gather | bytes 655360 | tf_op jit(solution)/shard_map/all_gather | solution.py:29
  60.0 14.6 %all_gather.109 = f32[4,2,128,128]{3,2,1,0:T(8,128)} all-gather(f32[1,2,128,128]{3,2,1,0:T(8,128)S(1)} %multiply_add_fusion.2), channel_id=1, replica_groups=mesh['sp_0'=4,'sp_1'=4,'sp_2'=2,'tp'=4] {'sp_0'}, dimensions={0}, use_global_device_ids=true | all-gather | bytes 655360 | tf_op jit(solution)/shard_map/all_gather | solution.py:29
  75.3 8.9 %all_gather.105 = f32[4,2,128]{2,1,0:T(2,128)S(1)} all-gather(f32[1,2,128]{2,1,0:T(2,128)S(1)} %copy-done.94), channel_id=1, replica_groups=mesh['sp_0'=4,'sp_1'=4,'sp_2'=2,'tp'=4] {'sp_0'}, dimensions={0}, use_global_device_ids=true | all-gather | bytes 5120 | tf_op jit(solution)/shard_map/all_gather | solution.py:29
  88.6 2.0 all-gather
  91.4 12.8 %all_gather.101 = f32[4,2,128,128]{3,2,1,0:T(8,128)S(1)} all-gather(f32[1,2,128,128]{3,2,1,0:T(8,128)S(1)} %bitcast_add_fusion.22), channel_id=1, replica_groups=mesh['sp_0'=4,'sp_1'=4,'sp_2'=2,'tp'=4] {'sp_1'}, dimensions={0}, use_global_device_ids=true | all-gather | bytes 655360 | tf_op jit(solution)/shard_map/all_gather | solution.py:29
  105.1 13.5 %all_gather.102 = f32[4,2,128,128]{3,2,1,0:T(8,128)} all-gather(f32[1,2,128,128]{3,2,1,0:T(8,128)S(1)} %multiply_add_fusion.3), channel_id=1, replica_groups=mesh['sp_0'=4,'sp_1'=4,'sp_2'=2,'tp'=4] {'sp_0'}, dimensions={0}, use_global_device_ids=true | all-gather | bytes 655360 | tf_op jit(solution)/shard_map/all_gather | solution.py:29
  119.3 7.1 %all_gather.98 = f32[4,2,128]{2,1,0:T(2,128)S(1)} all-gather(f32[1,2,128]{2,1,0:T(2,128)S(1)} %copy-done.93), channel_id=1, replica_groups=mesh['sp_0'=4,'sp_1'=4,'sp_2'=2,'tp'=4] {'sp_0'}, dimensions={0}, use_global_device_ids=true | all-gather | bytes 5120 | tf_op jit(solution)/shard_map/all_gather | solution.py:29
  129.5 1.6 fusion.49
  145.7 2.1 all-gather.3
  148.6 13.5 %all_gather.118 = f32[4,2,128,128]{3,2,1,0:T(8,128)S(1)} all-gather(f32[1,2,128,128]{3,2,1,0:T(8,128)S(1)} %bitcast_add_fusion.4), channel_id=1, replica_groups=mesh['sp_0'=4,'sp_1'=4,'sp_2'=2,'tp'=4] {'sp_1'}, dimensions={0}, use_global_device_ids=true | all-gather | bytes 655360 | tf_op jit(solution)/shard_map/all_gather | solution.py:29
  162.9 13.3 %all_gather.119 = f32[4,2,128,128]{3,2,1,0:T(8,128)S(1)} all-gather(f32[1,2,128,128]{3,2,1,0:T(8,128)S(1)} %multiply_add_fusion), channel_id=1, replica_groups=mesh['sp_0'=4,'sp_1'=4,'sp_2'=2,'tp'=4] {'sp_0'}, dimensions={0}, use_global_device_ids=true | all-gather | bytes 655360 | tf_op jit(solution)/shard_map/all_gather | solution.py:29
  176.9 8.3 %all_gather.115 = f32[4,2,128]{2,1,0:T(2,128)S(1)} all-gather(f32[1,2,128]{2,1,0:T(2,128)S(1)} %copy-done.92), channel_id=1, replica_groups=mesh['sp_0'=4,'sp_1'=4,'sp_2'=2,'tp'=4] {'sp_0'}, dimensions={0}, use_global_device_ids=true | all-gather | bytes 5120 | tf_op jit(solution)/shard_map/all_gather | solution.py:29
  188.2 2.0 all-gather.2
  191.0 12.9 %all_gather.113 = f32[4,2,128,128]{3,2,1,0:T(8,128)S(1)} all-gather(f32[1,2,128,128]{3,2,1,0:T(8,128)S(1)} %bitcast_add_fusion.10), channel_id=1, replica_groups=mesh['sp_0'=4,'sp_1'=4,'sp_2'=2,'tp'=4] {'sp_1'}, dimensions={0}, use_global_device_ids=true | all-gather | bytes 655360 | tf_op jit(solution)/shard_map/all_gather | solution.py:29
  204.8 12.8 %all_gather.114 = f32[4,2,128,128]{3,2,1,0:T(8,128)S(1)} all-gather(f32[1,2,128,128]{3,2,1,0:T(8,128)S(1)} %multiply_add_fusion.1), channel_id=1, replica_groups=mesh['sp_0'=4,'sp_1'=4,'sp_2'=2,'tp'=4] {'sp_0'}, dimensions={0}, use_global_device_ids=true | all-gather | bytes 655360 | tf_op jit(solution)/shard_map/all_gather | solution.py:29
  218.2 8.4 %all_gather.110 = f32[4,2,128]{2,1,0:T(2,128)S(1)} all-gather(f32[1,2,128]{2,1,0:T(2,128)S(1)} %copy-done.91), channel_id=1, replica_groups=mesh['sp_0'=4,'sp_1'=4,'sp_2'=2,'tp'=4] {'sp_0'}, dimensions={0}, use_global_device_ids=true | all-gather | bytes 5120 | tf_op jit(solution)/shard_map/all_gather | solution.py:29
  232.5 1.1 fusion.104
  233.7 1.4 fusion.175
  239.0 2.4 fusion.167
  246.6 1.4 copy.790
  250.0 8.5 %psum.21 = f32[2,256]{1,0:T(2,128)S(1)} all-reduce(f32[2,256]{1,0:T(2,128)S(1)} %bitcast.638), channel_id=1, replica_groups=mesh['sp_0'=4,'sp_1'=4,'sp_2'=2,'tp'=4] {'sp_0'}, use_global_device_ids=true, to_apply=%region_20.22 | all-reduce | flops 512 | bytes 4096 | tf_op jit(solution)/shard_map/psum | solution.py:46
  258.5 11.3 %psum.22 = f32[2,256]{1,0:T(2,128)S(1)} all-reduce(f32[2,256]{1,0:T(2,128)S(1)} %psum.21), channel_id=1, replica_groups=mesh['sp_0'=4,'sp_1'=4,'sp_2'=2,'tp'=4] {'sp_1'}, use_global_device_ids=true, to_apply=%region_21.23 | all-reduce | flops 512 | bytes 4096 | tf_op jit(solution)/shard_map/psum | solution.py:46
  269.8 2.5 psum.23
  272.9 1.5 convert_element_type.56
  274.4 75.2 %reduce-scatter.7.cloned.1.call-done = f32[32,256]{1,0:T(8,128)} async-done(((f32[1024,256]{1,0:T(8,128)}), f32[32,256]{1,0:T(8,128)}) %reduce-scatter.7.cloned.1.call-update) | async-done | bytes 32784
  (305 shorter events, 65.7 us)
Async XLA Ops:
  7.2 33.6 %copy-start = (bf16[1024,256]{1,0:T(8,128)(2,1)S(1)}, bf16[1024,256]{1,0:T(8,128)(2,1)}, u32[]{:S(2)}) copy-start(bf16[1024,256]{1,0:T(8,128)(2,1)} %param.10) | copy-start | bytes 1572868
  7.2 265.7 %reduce-scatter.5.cloned.1.call-start = ((), (), s32[]{:S(2)}) async-start(), calls=%async_computation.2 | async-start | bytes 655360 | tf_op jit(solution)/shard_map/reduce_scatter | solution.py:41
  8.6 3.0 copy-start.41
  8.6 5.5 %copy-start.39 = (f32[1,256]{1,0:T(1,128)}, f32[1,256]{1,0:T(1,128)S(1)}, u32[]{:S(2)}) copy-start(f32[1,256]{1,0:T(1,128)S(1)} %get-tuple-element.58) | copy-start | bytes 3076
  9.1 4.9 %copy-start.62 = (f32[2,128]{1,0:T(2,128)}, f32[2,128]{1,0:T(2,128)S(1)}, u32[]{:S(2)}) copy-start(f32[2,128]{1,0:T(2,128)S(1)} %get-tuple-element.149) | copy-start | bytes 3076
  9.1 2.1 copy-start.1
  9.1 2.1 copy-start.3
  11.5 1.6 copy-start.7
  14.0 28.2 %copy-start.47 = (f32[2,128]{1,0:T(2,128)}, f32[2,128]{1,0:T(2,128)S(1)}, u32[]{:S(2)}) copy-start(f32[2,128]{1,0:T(2,128)S(1)} %get-tuple-element.99) | copy-start | bytes 3076
  14.7 27.5 %copy-start.43 = (f32[2,128]{1,0:T(2,128)}, f32[2,128]{1,0:T(2,128)S(1)}, u32[]{:S(2)}) copy-start(f32[2,128]{1,0:T(2,128)S(1)} %get-tuple-element.97) | copy-start | bytes 3076
  17.1 29.1 %copy-start.56 = (f32[2,128]{1,0:T(2,128)}, f32[2,128]{1,0:T(2,128)S(1)}, u32[]{:S(2)}) copy-start(f32[2,128]{1,0:T(2,128)S(1)} %get-tuple-element.136) | copy-start | bytes 3076
  39.4 6.9 %copy-start.72 = (f32[2,128]{1,0:T(2,128)}, f32[2,128]{1,0:T(2,128)S(1)}, u32[]{:S(2)}) copy-start(f32[2,128]{1,0:T(2,128)S(1)} %get-tuple-element.134) | copy-start | bytes 3076
  43.6 41.3 %copy-start.9 = (f32[128,2,128]{2,1,0:T(2,128)}, f32[128,2,128]{2,1,0:T(2,128)S(1)}, u32[]{:S(2)}) copy-start(f32[128,2,128]{2,1,0:T(2,128)S(1)} %get-tuple-element.91) | copy-start | bytes 393220
  43.6 44.7 %copy-start.20 = (f32[128,2,128]{2,1,0:T(2,128)}, f32[128,2,128]{2,1,0:T(2,128)S(1)}, u32[]{:S(2)}) copy-start(f32[128,2,128]{2,1,0:T(2,128)S(1)} %get-tuple-element.94) | copy-start | bytes 393220
  46.4 12.8 %copy-start.58 = (f32[2,128]{1,0:T(2,128)S(1)}, f32[2,128]{1,0:T(2,128)}, u32[]{:S(2)}) copy-start(f32[2,128]{1,0:T(2,128)} %get-tuple-element.107) | copy-start | bytes 3076
  46.4 12.8 %copy-start.70 = (f32[2,128]{1,0:T(2,128)S(1)}, f32[2,128]{1,0:T(2,128)}, u32[]{:S(2)}) copy-start(f32[2,128]{1,0:T(2,128)} %get-tuple-element.112) | copy-start | bytes 3076
  88.6 2.0 copy-start.69
  91.4 12.8 %copy-start.68 = (f32[2,128]{1,0:T(2,128)S(1)}, f32[2,128]{1,0:T(2,128)}, u32[]{:S(2)}) copy-start(f32[2,128]{1,0:T(2,128)} %get-tuple-element.124) | copy-start | bytes 3076
  145.7 2.1 copy-start.67
  148.6 13.5 %copy-start.52 = (f32[2,128]{1,0:T(2,128)S(1)}, f32[2,128]{1,0:T(2,128)}, u32[]{:S(2)}) copy-start(f32[2,128]{1,0:T(2,128)} %get-tuple-element.110) | copy-start | bytes 3076
  148.6 13.5 %copy-start.66 = (f32[2,128]{1,0:T(2,128)S(1)}, f32[2,128]{1,0:T(2,128)}, u32[]{:S(2)}) copy-start(f32[2,128]{1,0:T(2,128)} %get-tuple-element.111) | copy-start | bytes 3076
  162.9 22.3 %copy-start.90 = (f32[2,128]{1,0:T(2,128)S(1)}, f32[2,128]{1,0:T(2,128)}, u32[]{:S(2)}) copy-start(f32[2,128]{1,0:T(2,128)} %get-tuple-element.64) | copy-start | bytes 3076
  188.2 2.0 copy-start.65
  191.0 12.9 %copy-start.64 = (f32[2,128]{1,0:T(2,128)S(1)}, f32[2,128]{1,0:T(2,128)}, u32[]{:S(2)}) copy-start(f32[2,128]{1,0:T(2,128)} %get-tuple-element.123) | copy-start | bytes 3076
  204.7 21.9 %copy-start.88 = (f32[2,128]{1,0:T(2,128)S(1)}, f32[2,128]{1,0:T(2,128)}, u32[]{:S(2)}) copy-start(f32[2,128]{1,0:T(2,128)} %get-tuple-element.70) | copy-start | bytes 3076
  233.7 1.5 copy-start.8
  233.7 1.5 copy-start.19
  236.8 1.5 copy-start.63
  236.8 1.5 copy-start.75
  239.0 2.4 copy-start.21
  239.0 2.4 copy-start.29
  246.2 103.4 %reduce-scatter.7.cloned.1.call-start = ((), (), s32[]{:S(2)}) async-start(), calls=%async_computation.3 | async-start | bytes 1081344
  (69 other events, 55.3 us)
Sparse Core Ops, SparseCore 0:
  246.3 22.3 reduce-scatter.4
  272.2 77.2 reduce-scatter.6
where the time goes:
time: 359 us; the launch traced here: 358 us
  blocking collectives  190 us (53%)
  waiting for transfers between devices  75.2 us (21%)
  local copies, waits for them, and re-layouts  31.1 us (9%)
  other arithmetic  28 us (8%)
  matrix products  18.7 us (5%)
  between operations  15.1 us (4%)
    all_gather x20, blocking collectives, entering(): pieces = jax.tree.map(lambda part: lax.all_gather(part, axis), subtotal)  168 us
    unnamed x3, waiting for transfers between devices  75.2 us
    unnamed x202, local copies, waits for them, and re-layouts  26.4 us
    psum x3, blocking collectives, one_axis_at_a_time(): array = lax.psum(array, axis)  22.3 us
  transfers between devices with their start and end apart: 2, of which 1 were waited for; matrix products, arithmetic and copies ran while one was open for 1% of the time, Pallas kernels for 0%

commit v1 on v0

v1 whole, which is shorter than its diff:
```python
import functools

import jax
import jax.numpy as jnp
from jax import lax
from jax.experimental import pallas as pl
from jax.experimental.pallas import tpu as pltpu
from jax.sharding import PartitionSpec as P

KDIM = 128
NORM_EPS = 1e-06
MESH = pl.DeviceIdType.MESH
F32 = jnp.float32
BF16 = jnp.bfloat16

NN = (((1,), (0,)), ((), ()))
NT = (((1,), (1,)), ((), ()))
TN = (((0,), (0,)), ((), ()))


def dot(a, b, dims):
    return lax.dot_general(a, b, dims, preferred_element_type=F32)


def split(a):
    high = a.astype(BF16)
    return high, (a - high.astype(F32)).astype(BF16)


def mm(a, b, dims):
    if not isinstance(a, tuple):
        return dot(a, b[0], dims) + dot(a, b[1], dims)
    if not isinstance(b, tuple):
        return dot(a[0], b, dims) + dot(a[1], b, dims)
    return dot(a[0], b[0], dims) + (dot(a[1], b[0], dims) + dot(a[0], b[1], dims))


def gates(raw, rate):
    opening = rate * (1.0 - rate * (0.5 - rate * (1.0 / 6.0 - rate * (1.0 / 24.0 - rate * (1.0 / 120.0)))))
    small = jnp.exp(-jnp.abs(raw))
    inverse = 1.0 / (1.0 + small)
    other = small * inverse
    positive = raw >= 0
    sig_pos = jnp.where(positive, inverse, other)
    sig_neg = jnp.where(positive, other, inverse)
    key = opening * sig_neg
    log_forget = -key * (1.0 + key * (0.5 + key * (1.0 / 3.0 + key * (0.25 + key * 0.2))))
    return key, log_forget, sig_pos, sig_neg, opening


def kernel(
    n_sp, n_tp, heads, seq_total,
    x_hbm, wq_hbm, wf_hbm, wb_hbm, wv_hbm, ct_hbm, rate_ref, gain_ref,
    gin_ref, gw_ref, gfl_ref,
    x_v, wq_v, wf_v, wb_v, wv_v, ct_v,
    dec_s, dec_r, a1_s, a1_r, a2_s, a2_r, b1_s, b1_r, b2_s, b2_r,
    w1_s, w1_r, w2_s, w2_r, y_s, rel_r, ysum_s, y_r, fl_s, fl_r,
    in_sem, snd, rcv, y_snd, y_rcv,
):
    me = lax.axis_index("sp")
    tp = lax.axis_index("tp")
    core = lax.rem(me, 2)
    chip = lax.div(me, 2)
    n_chip = n_sp // 2
    tok = x_hbm.shape[0]
    width = x_hbm.shape[1]
    per = n_sp // heads
    my_head = lax.div(me, per)
    q_scale = KDIM ** (-0.5)
    norm_scale = seq_total ** (-0.5)

    loads = [
        pltpu.make_async_copy(src, dst, in_sem.at[i])
        for i, (src, dst) in enumerate(
            [(x_hbm, x_v), (wf_hbm, wf_v), (wb_hbm, wb_v), (wv_hbm, wv_v), (wq_hbm, wq_v), (ct_hbm, ct_v)]
        )
    ]
    for load in loads:
        load.start()

    right = (me, lax.rem(tp + 1, n_tp))
    left = (me, lax.rem(tp + n_tp - 1, n_tp))
    barrier = pltpu.get_barrier_semaphore()

    def greet(r, c):
        pl.semaphore_signal(barrier, inc=1, device_id=(lax.rem(me + r, n_sp), tp), device_id_type=MESH)
        return c

    lax.fori_loop(1, n_sp, greet, 0)
    pl.semaphore_signal(barrier, inc=1, device_id=right, device_id_type=MESH)
    pl.semaphore_signal(barrier, inc=1, device_id=left, device_id_type=MESH)

    def spread(source_of, landing, i, count=n_sp, device_of=None):
        mine = me if count == n_sp else chip

        def step(r, c):
            to = lax.rem(mine + r, count)
            device = (to, tp) if count == n_sp else (to * 2 + core, tp)
            pltpu.make_async_remote_copy(
                src_ref=source_of(to), dst_ref=landing.at[count - r],
                send_sem=snd.at[i], recv_sem=rcv.at[i], device_id=device, device_id_type=MESH,
            ).start()
            return c

        lax.fori_loop(1, count, step, 0)

    def whole(landing, i, count=n_sp):
        part = landing.at[pl.ds(1, count - 1)]
        return pltpu.make_async_remote_copy(
            src_ref=part, dst_ref=part, send_sem=snd.at[i], recv_sem=rcv.at[i],
            device_id=(me, tp), device_id_type=MESH,
        )

    def place(j):
        return lax.rem(j - me + n_sp, n_sp)

    row = lax.broadcasted_iota(jnp.int32, (tok, tok), 0)
    col = lax.broadcasted_iota(jnp.int32, (tok, tok), 1)
    lower = col <= row
    upper = col >= row
    lower_ones = jnp.where(lower, 1.0, 0.0).astype(BF16)
    upper_ones = jnp.where(upper, 1.0, 0.0).astype(BF16)

    loads[0].wait()
    loads[1].wait()
    x = x_v[...]
    raw_f = dot(x, wf_v[...], NN).astype(BF16).astype(F32)
    loads[2].wait()
    raw_b = dot(x, wb_v[...], NN).astype(BF16).astype(F32)
    rate = rate_ref[...] * (1.0 / seq_total)
    key_f, log_f, sp_f, sn_f, open_f = gates(raw_f, rate[0:1])
    key_b, log_b, sp_b, sn_b, open_b = gates(raw_b, rate[1:2])
    cum_f = mm(lower_ones, split(log_f), NN)
    cum_b = mm(upper_ones, split(log_b), NN)
    dec_f = jnp.exp(cum_f[tok - 1 : tok])
    dec_b = jnp.exp(cum_b[0:1])
    head = lambda a, h: a[:, h * KDIM : (h + 1) * KDIM]
    for h in range(heads):
        dec_s[h, 0:1, :] = head(dec_f, h)
        dec_s[h, 1:2, :] = head(dec_b, h)
    pl.semaphore_wait(barrier, n_sp + 1)
    spread(lambda to: dec_s.at[lax.div(to, per)], dec_r, 0)
    dec_r[0] = dec_s[my_head]

    grow_f, grow_b = jnp.exp(-cum_f), jnp.exp(-cum_b)
    kd_f, kd_b = key_f * grow_f, key_b * grow_b
    kx_f, kx_b = kd_f * dec_f, kd_b * dec_b
    loads[3].wait()
    v = dot(x, wv_v[...], NN).astype(BF16)
    for h in range(heads):
        kx = split(jnp.concatenate([head(kx_f, h), head(kx_b, h)], axis=1))
        local = mm(head(v, h), kx, TN)
        a1_s[pl.ds(h * per, per), 0:8, :] = local[:, :KDIM].reshape(per, 8, KDIM)
        a1_s[pl.ds(h * per, per), 8:16, :] = local[:, KDIM:].reshape(per, 8, KDIM)

    spread(lambda to: a1_s.at[to], a1_r, 1)
    a1_r[0] = a1_s[me]

    loads[4].wait()
    q = dot(x, wq_v[...], NN).astype(BF16).astype(F32) * q_scale
    fade_f, fade_b = jnp.exp(cum_f), jnp.exp(cum_b)
    q_f, q_b = q * fade_f, q * fade_b
    q_fs = [split(head(q_f, h)) for h in range(heads)]
    q_bs = [split(head(q_b, h)) for h in range(heads)]
    kd_fs = [split(head(kd_f, h)) for h in range(heads)]
    kd_bs = [split(head(kd_b, h)) for h in range(heads)]
    scores = []
    inner = []
    for h in range(heads):
        score = jnp.where(lower, mm(q_fs[h], kd_fs[h], NT), 0.0) + jnp.where(upper, mm(q_bs[h], kd_bs[h], NT), 0.0)
        scores.append(split(score))
        inner.append(mm(scores[h], head(v, h), NN))

    def owner_scan(received, result, up_rows, up_dir, down_rows, down_dir):
        up = jnp.zeros((8, KDIM), F32)
        down = jnp.zeros((8, KDIM), F32)
        for i in range(n_sp):
            j, jj = i, n_sp - 1 - i
            slot, back = place(j), place(jj)
            result[j, up_rows, :] = up
            result[jj, down_rows, :] = down
            if i < n_sp - 1:
                up = up * dec_r[slot, up_dir : up_dir + 1, :] + received[slot, up_rows, :]
                down = down * dec_r[back, down_dir : down_dir + 1, :] + received[back, down_rows, :]

    FWD, BWD = slice(0, 8), slice(8, 16)

    def give_back(result, landing, i):
        def step(r, c):
            to = lax.rem(me + r, n_sp)
            pltpu.make_async_remote_copy(
                src_ref=result.at[to], dst_ref=landing.at[me],
                send_sem=snd.at[i], recv_sem=rcv.at[i], device_id=(to, tp), device_id_type=MESH,
            ).start()
            return c

        lax.fori_loop(1, n_sp, step, 0)
        landing[me] = result[me]

    whole(dec_r, 0).wait_recv()
    whole(a1_r, 1).wait_recv()
    owner_scan(a1_r, a2_s, FWD, 0, BWD, 1)
    give_back(a2_s, a2_r, 2)
    loads[5].wait()
    cot = ct_v[...].astype(F32)
    gain = gain_ref[...]
    whole(a2_r, 2).wait_recv()

    def state(buf, h, rows):
        return buf[pl.ds(h * per, per), rows, :].reshape(KDIM, KDIM)

    both = [split(jnp.concatenate([state(a2_r, h, FWD), state(a2_r, h, BWD)], axis=1)) for h in range(heads)]
    q_both = [tuple(jnp.concatenate([q_fs[h][i], q_bs[h][i]], axis=1) for i in range(2)) for h in range(heads)]
    d_out = []
    for h in range(heads):
        mixed = inner[h] + mm(q_both[h], both[h], NT)
        inv = lax.rsqrt(jnp.mean(mixed * mixed, axis=-1, keepdims=True) + NORM_EPS)
        scaled = head(cot, h) * gain
        pull = jnp.mean(mixed * scaled, axis=-1, keepdims=True)
        d_mixed = inv * scaled - mixed * (inv * inv * inv * pull)
        d_out.append(split(d_mixed))
        seed = mm(d_out[h], q_both[h], TN)
        b1_s[pl.ds(h * per, per), 0:8, :] = seed[:, :KDIM].reshape(per, 8, KDIM)
        b1_s[pl.ds(h * per, per), 8:16, :] = seed[:, KDIM:].reshape(per, 8, KDIM)
    spread(lambda to: b1_s.at[to], b1_r, 3)
    b1_r[0] = b1_s[me]

    dq_f, dq_b, d_low, d_high = [], [], [], []
    for h in range(heads):
        d_score = mm(d_out[h], head(v, h), NT)
        low = split(jnp.where(lower, d_score, 0.0))
        high = split(jnp.where(upper, d_score, 0.0))
        outer = mm(d_out[h], both[h], NN)
        dq_f.append(mm(low, kd_fs[h], NN) + outer[:, :KDIM])
        dq_b.append(mm(high, kd_bs[h], NN) + outer[:, KDIM:])
        d_low.append(low)
        d_high.append(high)
    cat = lambda parts: jnp.concatenate(parts, axis=1)
    dq_f, dq_b = cat(dq_f), cat(dq_b)
    g_q = ((dq_f * fade_f + dq_b * fade_b) * q_scale).astype(BF16)
    rows_w = width // n_sp
    for i in range(width // KDIM):
        block = dot(x_v[:, i * KDIM : (i + 1) * KDIM], g_q, TN)
        for k in range(KDIM // rows_w):
            p = i * (KDIM // rows_w) + k
            w1_s[p % 2, p // 2] = block[k * rows_w : (k + 1) * rows_w]
    sibling = pltpu.make_async_remote_copy(
        src_ref=w1_s.at[1 - core], dst_ref=w1_r, send_sem=snd.at[5], recv_sem=rcv.at[5],
        device_id=(me + 1 - 2 * core, tp), device_id_type=MESH,
    )
    sibling.start()
    dk_f = cat([mm(d_low[h], q_fs[h], TN) for h in range(heads)])
    dk_b = cat([mm(d_high[h], q_bs[h], TN) for h in range(heads)])
    dv = [mm(scores[h], d_out[h], TN) for h in range(heads)]

    whole(b1_r, 3).wait_recv()
    owner_scan(b1_r, b2_s, BWD, 1, FWD, 0)
    give_back(b2_s, b2_r, 4)

    sibling.wait_recv()
    w2_s[...] = w1_s[core] + w1_r[...]
    spread(lambda to: w2_s.at[to], w2_r, 6, n_chip)

    whole(b2_r, 4).wait_recv()
    dx_f, dx_b, edge_f, edge_b = [], [], [], []
    for h in range(heads):
        back_f, back_b = state(b2_r, h, FWD), state(b2_r, h, BWD)
        back = split(jnp.concatenate([back_f, back_b], axis=1))
        dx = mm(head(v, h), back, NN)
        dx_f.append(dx[:, :KDIM])
        dx_b.append(dx[:, KDIM:])
        kx = split(jnp.concatenate([head(kx_f, h), head(kx_b, h)], axis=1))
        dv[h] = dv[h] + mm(kx, back, NT)
        leave_f = head(dec_f, h) * state(a2_r, h, FWD) + state(a1_s, h, FWD)
        leave_b = head(dec_b, h) * state(a2_r, h, BWD) + state(a1_s, h, BWD)
        edge_f.append(jnp.sum(leave_f * back_f, axis=0, keepdims=True))
        edge_b.append(jnp.sum(leave_b * back_b, axis=0, keepdims=True))
    dx_f, dx_b, edge_f, edge_b = cat(dx_f), cat(dx_b), cat(edge_f), cat(edge_b)

    def gate_back(dk, dx, dq, kd, kx, q_d, grow, dec, edge, ones, key, sig_pos, sig_neg, opening):
        along = q_d * dq - kd * dk - kx * dx
        d_log = mm(ones, split(along), NN) + edge
        d_key = grow * (dk + dec * dx) - d_log / (1.0 - key)
        d_raw = -d_key * key * sig_pos
        d_rate = jnp.sum(d_key * sig_neg, axis=0, keepdims=True) * ((1.0 - opening) * (1.0 / seq_total))
        return d_raw.astype(BF16), d_rate

    g_f, r_f = gate_back(dk_f, dx_f, dq_f, kd_f, kx_f, q_f, grow_f, dec_f, edge_f, upper_ones, key_f, sp_f, sn_f, open_f)
    g_b, r_b = gate_back(dk_b, dx_b, dq_b, kd_b, kx_b, q_b, grow_b, dec_b, edge_b, lower_ones, key_b, sp_b, sn_b, open_b)
    g_v = cat(dv).astype(BF16)
    for h in range(heads):
        fl_s[h : h + 1, :] = head(r_f, h)
        fl_s[heads + h : heads + h + 1, :] = head(r_b, h)
    spread(lambda to: fl_s, fl_r, 7)
    fl_r[0] = fl_s[...]

    rows_y = tok // n_tp
    half = width // 2
    for part in range(2):
        cols = pl.ds(part * half, half)
        y = (
            dot(g_q, wq_v[cols, :], NT)
            + dot(g_f, wf_v[cols, :], NT)
            + dot(g_b, wb_v[cols, :], NT)
            + dot(g_v, wv_v[cols, :], NT)
        )
        y_s[part] = y.reshape(n_tp, rows_y, half)

    up, down, across = lax.rem(tp + 1, n_tp), lax.rem(tp + n_tp - 1, n_tp), lax.rem(tp + 2, n_tp)

    def ring(src, dst, i, device):
        return pltpu.make_async_remote_copy(
            src_ref=src, dst_ref=dst, send_sem=y_snd.at[i], recv_sem=y_rcv.at[i],
            device_id=device, device_id_type=MESH,
        )

    hops = [
        ring(y_s.at[0, across], rel_r.at[0], 0, right),
        ring(y_s.at[1, across], rel_r.at[1], 1, left),
        ring(y_s.at[1, up], y_r.at[0], 2, right),
        ring(y_s.at[0, down], y_r.at[1], 3, left),
        ring(ysum_s.at[0], y_r.at[2], 4, right),
        ring(ysum_s.at[1], y_r.at[3], 5, left),
    ]
    for hop in hops[:4]:
        hop.start()
    hops[0].wait_recv()
    ysum_s[0] = y_s[0, up] + rel_r[0]
    hops[4].start()
    hops[1].wait_recv()
    ysum_s[1] = y_s[1, down] + rel_r[1]
    hops[5].start()

    whole(fl_r, 7).wait_recv()
    total = jnp.zeros((2 * heads, KDIM), F32)
    for j in range(n_sp):
        total = total + fl_r[place(j)]
    total = total * norm_scale
    for h in range(heads):
        gfl_ref[0:1, h * KDIM : (h + 1) * KDIM] = total[h : h + 1]
        gfl_ref[1:2, h * KDIM : (h + 1) * KDIM] = total[heads + h : heads + h + 1]

    whole(w2_r, 6, n_chip).wait_recv()
    acc = w2_s[chip]
    for r in range(1, n_chip):
        acc = acc + w2_r[r]
    gw_ref[...] = acc * norm_scale

    for hop in hops[2:]:
        hop.wait_recv()
    gin_ref[:, 0:half] = (y_s[0, tp] + y_r[2] + y_r[1]).astype(BF16)
    gin_ref[:, half:] = (y_s[1, tp] + y_r[0] + y_r[3]).astype(BF16)

    for landing, i in ((dec_r, 0), (a1_r, 1), (a2_r, 2), (b1_r, 3), (b2_r, 4), (fl_r, 7)):
        whole(landing, i).wait_send()
    whole(w2_r, 6, n_chip).wait_send()
    sibling.wait_send()
    for hop in hops:
        hop.wait_send()


def solution(mesh):
    n_sp, n_tp = mesh.shape["sp"], mesh.shape["tp"]

    def body(block_input, w_query, w_forget_fwd, w_forget_bwd, w_value, floor_rate, gain, cotangent):
        tok, width = block_input.shape
        cols = w_query.shape[1]
        heads = cols // KDIM
        n_chip = n_sp // 2
        rows_w = width // n_sp
        rows_y = tok // n_tp
        half = width // 2
        vm = pltpu.VMEM
        pieces = [vm((n_sp, 16, KDIM), F32) for _ in range(8)]
        any_spec = pl.BlockSpec(memory_space=pl.ANY)
        vmem_spec = pl.BlockSpec(memory_space=pltpu.VMEM)
        return pl.pallas_call(
            functools.partial(kernel, n_sp, n_tp, heads, float(tok * n_sp)),
            out_shape=(
                jax.ShapeDtypeStruct((rows_y, width), BF16),
                jax.ShapeDtypeStruct((rows_w, cols), F32),
                jax.ShapeDtypeStruct((2, cols), F32),
            ),
            in_specs=[any_spec] * 6 + [vmem_spec] * 2,
            out_specs=(vmem_spec,) * 3,
            scratch_shapes=[
                vm((tok, width), BF16),
                vm((width, cols), BF16), vm((width, cols), BF16), vm((width, cols), BF16), vm((width, cols), BF16),
                vm((tok, cols), BF16),
                vm((heads, 2, KDIM), F32), vm((n_sp, 2, KDIM), F32),
                *pieces,
                vm((2, n_chip, rows_w, cols), F32), vm((n_chip, rows_w, cols), F32),
                vm((n_chip, rows_w, cols), F32), vm((n_chip, rows_w, cols), F32),
                vm((2, n_tp, rows_y, half), F32), vm((2, rows_y, half), F32),
                vm((2, rows_y, half), F32), vm((4, rows_y, half), F32),
                vm((2 * heads, KDIM), F32), vm((n_sp, 2 * heads, KDIM), F32),
                pltpu.SemaphoreType.DMA((6,)),
                pltpu.SemaphoreType.DMA((8,)),
                pltpu.SemaphoreType.DMA((8,)),
                pltpu.SemaphoreType.DMA((6,)),
                pltpu.SemaphoreType.DMA((6,)),
            ],
            compiler_params=pltpu.CompilerParams(collective_id=0, has_side_effects=True),
        )(block_input, w_query, w_forget_fwd, w_forget_bwd, w_value, cotangent, floor_rate, gain.reshape(1, KDIM))

    return jax.shard_map(
        body,
        mesh=mesh,
        in_specs=(
            P("sp", None), P(None, "tp"), P(None, "tp"), P(None, "tp"), P(None, "tp"), P(None, "tp"), P(), P("sp", "tp"),
        ),
        out_specs=(P(("sp", "tp"), None), P("sp", "tp"), P(None, "tp")),
        check_vma=False,
    )
```

time: 359 us -> 49.4 us (0.14)
  blocking collectives: 190 us -> 0 us
  waiting for transfers between devices: 75.2 us -> 0 us
  Pallas kernels: 0 us -> 45.8 us
  local copies, waits for them, and re-layouts: 31.1 us -> 2.74 us
  other arithmetic: 28 us -> 0 us
  matrix products: 18.7 us -> 0 us
  between operations: 15.1 us -> 0.65 us
    all_gather x20 -> x0, blocking collectives: 168 us -> none  [entering(): pieces = jax.tree.map(lambda part: lax.all_gather(part, axis), subtotal)]
    unnamed x3 -> x0, waiting for transfers between devices: 75.2 us -> none
    pallas_call x0 -> x1, Pallas kernels: none -> 45.8 us  [body(): pl.pallas_call(functools.partial(kernel, n_sp, n_tp, heads, float(tok * n...]
    unnamed x202 -> x7, local copies, waits for them, and re-layouts: 26.4 us -> 2.74 us
    psum x3 -> x0, blocking collectives: 22.3 us -> none  [one_axis_at_a_time(): array = lax.psum(array, axis)]
    dot_general x33 -> x0, matrix products: 18.7 us -> none  [the longest x6 4.19 us: span_output(): jnp.einsum('nea,eaw->new', faded_asking_vector, arriving_signal, precisio...]
    mul x14 -> x0, other arithmetic: 7.66 us -> none  [the longest x10 4.85 us: compose(): return (earlier[0] * later[0], later[0][..., None] * earlier[1] + later[1])]
    another operation x6 -> x0, other arithmetic: 6.87 us -> none  [the longest x4 4.58 us: span_output(): cumul = jnp.cumsum(log_forget, axis=0)]
  transfers between devices with their start and end apart: 2 -> 0, of which waited for: 1 -> 0; matrix products, arithmetic and copies ran while one was open for 1% -> 0% of each run, Pallas kernels for 0% -> 0%
where the time goes in v1:
time: 49.4 us; the launch traced here: 49.2 us
  Pallas kernels  45.8 us (93%)
  local copies, waits for them, and re-layouts  2.74 us (6%)
  between operations  0.65 us (1%)
    pallas_call x1, Pallas kernels, body(): pl.pallas_call(functools.partial(kernel, n_sp, n_tp, heads, float(tok * n...  45.8 us
    unnamed x7, local copies, waits for them, and re-layouts  2.74 us

profile of v1, /device:TPU:0, one launch (start us, length us, event | category | flops | bytes accessed | tf_op | source)
XLA Modules:
  0.0 49.2 jit_solution(408975128694211379)
XLA Ops:
  0.6 45.8 %shard_map.103 = (bf16[32,1024]{1,0:T(8,128)(2,1)}, f32[32,256]{1,0:T(8,128)}, f32[2,256]{1,0:T(2,128)}) custom-call(bf16[128,1024]{1,0:T(8,128)(2,1)} %x_hbm.1, bf16[1024,256]{1,0:T(8,128)(2,1)} %wq_hbm.1, bf16[1024,256]{1,0:T(8,128)(2,1)} %wf_hbm.1, bf16[1024,256]{1,0:T(8,128)(2,1)} %wb_hbm.1, bf16[1024,256]{1,0:T(8,128)(2,1)} %wv_hbm.1, ...), custom_call_target="tpu_custom_call" | custom-call | tf_op jit(solution)/shard_map/pallas_call | solution.py:377
  46.4 0.0 copy-start
  46.4 1.5 %copy.14 = bf16[32,1024]{1,0:T(8,128)(2,1)} copy(bf16[32,1024]{1,0:T(8,128)(2,1)} %get-tuple-element.6) | data formatting | bytes 131072
  47.9 0.0 copy-done
  47.9 0.0 copy-start.1
  47.9 0.6 %copy.15 = f32[32,256]{1,0:T(8,128)} copy(f32[32,256]{1,0:T(8,128)S(1)} %copy-done) | data formatting | bytes 65536
  48.5 0.1 copy-done.1
  48.6 0.6 %copy.16 = f32[2,256]{1,0:T(2,128)} copy(f32[2,256]{1,0:T(2,128)S(1)} %copy-done.1) | data formatting | bytes 4096
Async XLA Ops:
  46.4 1.5 %copy-start = (f32[32,256]{1,0:T(8,128)S(1)}, f32[32,256]{1,0:T(8,128)}, u32[]{:S(2)}) copy-start(f32[32,256]{1,0:T(8,128)} %get-tuple-element.7) | copy-start | bytes 98308
  47.9 0.7 %copy-start.1 = (f32[2,256]{1,0:T(2,128)S(1)}, f32[2,256]{1,0:T(2,128)}, u32[]{:S(2)}) copy-start(f32[2,256]{1,0:T(2,128)} %get-tuple-element.8) | copy-start | bytes 6148

commit v2 on v1

v2 whole, which is shorter than its diff:
```python
import functools

import jax
import jax.numpy as jnp
from jax import lax
from jax.experimental import pallas as pl
from jax.experimental.pallas import tpu as pltpu
from jax.sharding import PartitionSpec as P

KDIM = 128
NORM_EPS = 1e-06
MESH = pl.DeviceIdType.MESH
F32 = jnp.float32
BF16 = jnp.bfloat16

NN = (((1,), (0,)), ((), ()))
NT = (((1,), (1,)), ((), ()))
TN = (((0,), (0,)), ((), ()))


def dot(a, b, dims):
    return lax.dot_general(a, b, dims, preferred_element_type=F32)


def split(a):
    high = a.astype(BF16)
    return high, (a - high.astype(F32)).astype(BF16)


def mm(a, b, dims):
    if not isinstance(a, tuple):
        return dot(a, b[0], dims) + dot(a, b[1], dims)
    if not isinstance(b, tuple):
        return dot(a[0], b, dims) + dot(a[1], b, dims)
    return dot(a[0], b[0], dims) + (dot(a[1], b[0], dims) + dot(a[0], b[1], dims))


def gates(raw, rate):
    opening = rate * (1.0 - rate * (0.5 - rate * (1.0 / 6.0 - rate * (1.0 / 24.0 - rate * (1.0 / 120.0)))))
    small = jnp.exp(-jnp.abs(raw))
    inverse = 1.0 / (1.0 + small)
    other = small * inverse
    positive = raw >= 0
    sig_pos = jnp.where(positive, inverse, other)
    sig_neg = jnp.where(positive, other, inverse)
    key = opening * sig_neg
    log_forget = -key * (1.0 + key * (0.5 + key * (1.0 / 3.0 + key * (0.25 + key * 0.2))))
    return key, log_forget, sig_pos, sig_neg, opening


def kernel(
    n_sp, n_tp, heads, seq_total,
    x_hbm, wq_hbm, wf_hbm, wb_hbm, wv_hbm, ct_hbm, rate_ref, gain_ref,
    gin_ref, gw_ref, gfl_ref,
    x_v, wq_v, wf_v, wb_v, wv_v, ct_v,
    dec_s, dec_r, a1_s, a1_r, a2_s, a2_r, b1_s, b1_r, b2_s, b2_r,
    w1_s, w1_r, w2_s, w2_r, y_s, rel_r, ysum_s, y_r, fl_s, fl_r,
    in_sem, snd, rcv, y_snd, y_rcv,
):
    me = lax.axis_index("sp")
    tp = lax.axis_index("tp")
    core = lax.rem(me, 2)
    chip = lax.div(me, 2)
    n_chip = n_sp // 2
    tok = x_hbm.shape[0]
    width = x_hbm.shape[1]
    per = n_sp // heads
    my_head = lax.div(me, per)
    q_scale = KDIM ** (-0.5)
    norm_scale = seq_total ** (-0.5)

    loads = [
        pltpu.make_async_copy(src, dst, in_sem.at[i])
        for i, (src, dst) in enumerate(
            [(x_hbm, x_v), (wf_hbm, wf_v), (wb_hbm, wb_v), (wv_hbm, wv_v), (wq_hbm, wq_v), (ct_hbm, ct_v)]
        )
    ]
    for load in loads:
        load.start()
    loading = dict(enumerate(loads))
    flying, sent = {}, []

    def loaded(i):
        loading.pop(i).wait()

    def begun(name, copy):
        flying[name] = copy
        sent.append(copy)

    def arrived(name):
        flying.pop(name).wait_recv()

    def drain():
        for name in list(flying):
            arrived(name)
        for i in list(loading):
            loaded(i)
        for copy in sent:
            copy.wait_send()

    right = (me, lax.rem(tp + 1, n_tp))
    left = (me, lax.rem(tp + n_tp - 1, n_tp))
    barrier = pltpu.get_barrier_semaphore()

    def greet(r, c):
        pl.semaphore_signal(barrier, inc=1, device_id=(lax.rem(me + r, n_sp), tp), device_id_type=MESH)
        return c

    lax.fori_loop(1, n_sp, greet, 0)
    pl.semaphore_signal(barrier, inc=1, device_id=right, device_id_type=MESH)
    pl.semaphore_signal(barrier, inc=1, device_id=left, device_id_type=MESH)

    def put(src, dst, i, device):
        pltpu.make_async_remote_copy(
            src_ref=src, dst_ref=dst, send_sem=snd.at[i], recv_sem=rcv.at[i],
            device_id=device, device_id_type=MESH,
        ).start()

    def took(part, i):
        return pltpu.make_async_remote_copy(
            src_ref=part, dst_ref=part, send_sem=snd.at[i], recv_sem=rcv.at[i],
            device_id=(me, tp), device_id_type=MESH,
        )

    def to_all(source_of, landing, i):
        def step(r, c):
            to = lax.rem(me + r, n_sp)
            put(source_of(to), landing.at[me], i, (to, tp))
            return c

        lax.fori_loop(1, n_sp, step, 0)
        begun(i, took(landing.at[pl.ds(0, n_sp - 1)], i))

    def to_owners(source, landing, i, h):
        mine = lax.rem(me, per)

        def step(r, c):
            to = h * per + lax.rem(mine + r, per)
            put(source.at[to], landing.at[me], i, (to, tp))
            return c

        lax.fori_loop(jnp.where(my_head == h, 1, 0), per, step, 0)
        if h == heads - 1:
            begun(i, took(landing.at[pl.ds(0, n_sp - 1)], i))
            landing[me] = source[me]

    def give_back(result, landing, i):
        def step(r, c):
            to = lax.rem(me + r, n_sp)
            pltpu.make_async_remote_copy(
                src_ref=result.at[to], dst_ref=landing.at[me], send_sem=snd.at[i], recv_sem=rcv.at[i + my_head],
                device_id=(to, tp), device_id_type=MESH,
            ).start()
            return c

        lax.fori_loop(1, n_sp, step, 0)
        sent.append(took(landing.at[pl.ds(0, n_sp - 1)], i))
        landing[me] = result[me]

    def head_arrived(landing, i, h):
        @pl.when(my_head == h)
        def _():
            took(landing.at[pl.ds(h * per, per - 1)], i + h).wait_recv()

        @pl.when(my_head != h)
        def _():
            took(landing.at[pl.ds(h * per, per)], i + h).wait_recv()

    row = lax.broadcasted_iota(jnp.int32, (tok, tok), 0)
    col = lax.broadcasted_iota(jnp.int32, (tok, tok), 1)
    lower = col <= row
    upper = col >= row
    lower_ones = jnp.where(lower, 1.0, 0.0).astype(BF16)
    upper_ones = jnp.where(upper, 1.0, 0.0).astype(BF16)

    loaded(0)
    loaded(1)
    x = x_v[...]
    raw_f = dot(x, wf_v[...], NN).astype(BF16).astype(F32)
    loaded(2)
    raw_b = dot(x, wb_v[...], NN).astype(BF16).astype(F32)
    rate = rate_ref[...] * (1.0 / seq_total)
    key_f, log_f, sp_f, sn_f, open_f = gates(raw_f, rate[0:1])
    key_b, log_b, sp_b, sn_b, open_b = gates(raw_b, rate[1:2])
    cum_f = mm(lower_ones, split(log_f), NN)
    cum_b = mm(upper_ones, split(log_b), NN)
    dec_f = jnp.exp(cum_f[tok - 1 : tok])
    dec_b = jnp.exp(cum_b[0:1])
    head = lambda a, h: a[:, h * KDIM : (h + 1) * KDIM]
    for h in range(heads):
        dec_s[h, 0:1, :] = head(dec_f, h)
        dec_s[h, 1:2, :] = head(dec_b, h)
    dec_r[me] = dec_s[my_head]

    grow_f, grow_b = jnp.exp(-cum_f), jnp.exp(-cum_b)
    kd_f, kd_b = key_f * grow_f, key_b * grow_b
    kx_f, kx_b = kd_f * dec_f, kd_b * dec_b
    loaded(3)
    v = dot(x, wv_v[...], NN).astype(BF16)
    for h in range(heads):
        kx = split(jnp.concatenate([head(kx_f, h), head(kx_b, h)], axis=1))
        local = mm(head(v, h), kx, TN)
        a1_s[pl.ds(h * per, per), 0:8, :] = local[:, :KDIM].reshape(per, 8, KDIM)
        a1_s[pl.ds(h * per, per), 8:16, :] = local[:, KDIM:].reshape(per, 8, KDIM)

    pl.semaphore_wait(barrier, n_sp + 1)
    for h in range(heads):
        to_owners(a1_s, a1_r, 1, h)
    to_all(lambda to: dec_s.at[lax.div(to, per)], dec_r, 0)

    loaded(4)
    q = dot(x, wq_v[...], NN).astype(BF16).astype(F32) * q_scale
    fade_f, fade_b = jnp.exp(cum_f), jnp.exp(cum_b)
    q_f, q_b = q * fade_f, q * fade_b
    q_fs = [split(head(q_f, h)) for h in range(heads)]
    q_bs = [split(head(q_b, h)) for h in range(heads)]
    kd_fs = [split(head(kd_f, h)) for h in range(heads)]
    kd_bs = [split(head(kd_b, h)) for h in range(heads)]
    scores = []
    inner = []
    for h in range(heads):
        score = jnp.where(lower, mm(q_fs[h], kd_fs[h], NT), 0.0) + jnp.where(upper, mm(q_bs[h], kd_bs[h], NT), 0.0)
        scores.append(split(score))
        inner.append(mm(scores[h], head(v, h), NN))

    def owner_scan(received, result, up_rows, up_dir, down_rows, down_dir):
        up = jnp.zeros((8, KDIM), F32)
        down = jnp.zeros((8, KDIM), F32)
        for j in range(n_sp):
            k = n_sp - 1 - j
            result[j, up_rows, :] = up
            result[k, down_rows, :] = down
            if j < n_sp - 1:
                up = up * dec_r[j, up_dir : up_dir + 1, :] + received[j, up_rows, :]
                down = down * dec_r[k, down_dir : down_dir + 1, :] + received[k, down_rows, :]

    FWD, BWD = slice(0, 8), slice(8, 16)

    arrived(0)
    arrived(1)
    owner_scan(a1_r, a2_s, FWD, 0, BWD, 1)
    give_back(a2_s, a2_r, 2)
    loaded(5)
    cot = ct_v[...].astype(F32)
    gain = gain_ref[...]
    def state(buf, h, rows):
        return buf[pl.ds(h * per, per), rows, :].reshape(KDIM, KDIM)

    q_both = [tuple(jnp.concatenate([q_fs[h][i], q_bs[h][i]], axis=1) for i in range(2)) for h in range(heads)]
    both, d_out = [], []
    for h in range(heads):
        head_arrived(a2_r, 2, h)
        both.append(split(jnp.concatenate([state(a2_r, h, FWD), state(a2_r, h, BWD)], axis=1)))
        mixed = inner[h] + mm(q_both[h], both[h], NT)
        inv = lax.rsqrt(jnp.mean(mixed * mixed, axis=-1, keepdims=True) + NORM_EPS)
        scaled = head(cot, h) * gain
        pull = jnp.mean(mixed * scaled, axis=-1, keepdims=True)
        d_mixed = inv * scaled - mixed * (inv * inv * inv * pull)
        d_out.append(split(d_mixed))
        seed = mm(d_out[h], q_both[h], TN)
        b1_s[pl.ds(h * per, per), 0:8, :] = seed[:, :KDIM].reshape(per, 8, KDIM)
        b1_s[pl.ds(h * per, per), 8:16, :] = seed[:, KDIM:].reshape(per, 8, KDIM)
        to_owners(b1_s, b1_r, 4, h)

    dq_f, dq_b, d_low, d_high = [], [], [], []
    for h in range(heads):
        d_score = mm(d_out[h], head(v, h), NT)
        low = split(jnp.where(lower, d_score, 0.0))
        high = split(jnp.where(upper, d_score, 0.0))
        outer = mm(d_out[h], both[h], NN)
        dq_f.append(mm(low, kd_fs[h], NN) + outer[:, :KDIM])
        dq_b.append(mm(high, kd_bs[h], NN) + outer[:, KDIM:])
        d_low.append(low)
        d_high.append(high)
    cat = lambda parts: jnp.concatenate(parts, axis=1)
    g_q = ((cat(dq_f) * fade_f + cat(dq_b) * fade_b) * q_scale).astype(BF16)
    rows_w = width // n_sp
    for i in range(width // KDIM):
        block = dot(x_v[:, i * KDIM : (i + 1) * KDIM], g_q, TN)
        for k in range(KDIM // rows_w):
            p = i * (KDIM // rows_w) + k
            w1_s[p % 2, p // 2] = block[k * rows_w : (k + 1) * rows_w]
    sibling = pltpu.make_async_remote_copy(
        src_ref=w1_s.at[1 - core], dst_ref=w1_r, send_sem=snd.at[7], recv_sem=rcv.at[7],
        device_id=(me + 1 - 2 * core, tp), device_id_type=MESH,
    )
    sibling.start()
    begun(7, sibling)
    dk_f = [mm(d_low[h], q_fs[h], TN) for h in range(heads)]
    dk_b = [mm(d_high[h], q_bs[h], TN) for h in range(heads)]
    dv = [mm(scores[h], d_out[h], TN) for h in range(heads)]
    quarter = width // 4
    rows_y = tok // n_tp
    for c in range(4):
        y_s[c] = dot(g_q, wq_v[c * quarter : (c + 1) * quarter, :], NT).reshape(n_tp, rows_y, quarter)

    arrived(4)
    owner_scan(b1_r, b2_s, BWD, 1, FWD, 0)
    give_back(b2_s, b2_r, 5)

    arrived(7)
    w2_s[...] = w1_s[core] + w1_r[...]

    def to_chip(r, c):
        to = lax.rem(chip + r, n_chip)
        put(w2_s.at[to], w2_r.at[n_chip - r], 8, (to * 2 + core, tp))
        return c

    lax.fori_loop(1, n_chip, to_chip, 0)
    begun(8, took(w2_r.at[pl.ds(1, n_chip - 1)], 8))

    def gate_back(dk, dx, dq, kd, kx, q_d, grow, dec, edge, ones, key, sig_pos, sig_neg, opening):
        along = q_d * dq - kd * dk - kx * dx
        d_log = mm(ones, split(along), NN) + edge
        d_key = grow * (dk + dec * dx) - d_log / (1.0 - key)
        d_raw = -d_key * key * sig_pos
        d_rate = jnp.sum(d_key * sig_neg, axis=0, keepdims=True) * ((1.0 - opening) * (1.0 / seq_total))
        return d_raw.astype(BF16), d_rate

    for h in range(heads):
        head_arrived(b2_r, 5, h)
        back_f, back_b = state(b2_r, h, FWD), state(b2_r, h, BWD)
        back = split(jnp.concatenate([back_f, back_b], axis=1))
        dx = mm(head(v, h), back, NN)
        kx = split(jnp.concatenate([head(kx_f, h), head(kx_b, h)], axis=1))
        g_v = (dv[h] + mm(kx, back, NT)).astype(BF16)
        leave_f = head(dec_f, h) * state(a2_r, h, FWD) + state(a1_s, h, FWD)
        leave_b = head(dec_b, h) * state(a2_r, h, BWD) + state(a1_s, h, BWD)
        edge_f = jnp.sum(leave_f * back_f, axis=0, keepdims=True)
        edge_b = jnp.sum(leave_b * back_b, axis=0, keepdims=True)
        here = lambda *arrays: [head(a, h) for a in arrays]
        g_f, r_f = gate_back(
            dk_f[h], dx[:, :KDIM], dq_f[h], *here(kd_f, kx_f, q_f, grow_f, dec_f), edge_f,
            upper_ones, *here(key_f, sp_f, sn_f, open_f),
        )
        g_b, r_b = gate_back(
            dk_b[h], dx[:, KDIM:], dq_b[h], *here(kd_b, kx_b, q_b, grow_b, dec_b), edge_b,
            lower_ones, *here(key_b, sp_b, sn_b, open_b),
        )
        fl_s[h : h + 1, :] = r_f
        fl_s[heads + h : heads + h + 1, :] = r_b
        mine = slice(h * KDIM, (h + 1) * KDIM)
        for c in range(4):
            rows = slice(c * quarter, (c + 1) * quarter)
            y = (
                dot(g_f, wf_v[rows, mine], NT)
                + dot(g_b, wb_v[rows, mine], NT)
                + dot(g_v, wv_v[rows, mine], NT)
            )
            y_s[c] = y_s[c] + y.reshape(n_tp, rows_y, quarter)

    up, down, across = lax.rem(tp + 1, n_tp), lax.rem(tp + n_tp - 1, n_tp), lax.rem(tp + 2, n_tp)

    def ring(src, dst, i, device):
        return pltpu.make_async_remote_copy(
            src_ref=src, dst_ref=dst, send_sem=y_snd.at[i], recv_sem=y_rcv.at[i],
            device_id=device, device_id_type=MESH,
        )

    relay, direct, summed = [], [], []
    for c in range(4):
        ahead, behind = (right, left) if c % 2 == 0 else (left, right)
        relay.append(ring(y_s.at[c, across], rel_r.at[c], c, ahead))
        direct.append(ring(y_s.at[c, down if c % 2 == 0 else up], y_r.at[c], 4 + c, behind))
        summed.append(ring(ysum_s.at[c], y_r.at[4 + c], 8 + c, ahead))
    for c in range(4):
        relay[c].start()
        begun(("relay", c), relay[c])
    for c in range(4):
        direct[c].start()
        begun(("direct", c), direct[c])
    to_all(lambda to: fl_s, fl_r, 9)
    fl_r[me] = fl_s[...]
    for c in range(4):
        arrived(("relay", c))
        ysum_s[c] = y_s[c, up if c % 2 == 0 else down] + rel_r[c]
        summed[c].start()
        begun(("summed", c), summed[c])

    arrived(9)
    total = fl_r[0]
    for j in range(1, n_sp):
        total = total + fl_r[j]
    total = total * norm_scale
    for h in range(heads):
        gfl_ref[0:1, h * KDIM : (h + 1) * KDIM] = total[h : h + 1]
        gfl_ref[1:2, h * KDIM : (h + 1) * KDIM] = total[heads + h : heads + h + 1]

    arrived(8)
    acc = w2_s[chip]
    for r in range(1, n_chip):
        acc = acc + w2_r[r]
    gw_ref[...] = acc * norm_scale

    for c in range(4):
        arrived(("direct", c))
        arrived(("summed", c))
        gin_ref[:, c * quarter : (c + 1) * quarter] = (y_s[c, tp] + y_r[c] + y_r[4 + c]).astype(BF16)

    drain()


def solution(mesh):
    n_sp, n_tp = mesh.shape["sp"], mesh.shape["tp"]

    def body(block_input, w_query, w_forget_fwd, w_forget_bwd, w_value, floor_rate, gain, cotangent):
        tok, width = block_input.shape
        cols = w_query.shape[1]
        heads = cols // KDIM
        n_chip = n_sp // 2
        rows_w = width // n_sp
        rows_y = tok // n_tp
        quarter = width // 4
        vm = pltpu.VMEM
        pieces = [vm((n_sp, 16, KDIM), F32) for _ in range(8)]
        any_spec = pl.BlockSpec(memory_space=pl.ANY)
        vmem_spec = pl.BlockSpec(memory_space=pltpu.VMEM)
        return pl.pallas_call(
            functools.partial(kernel, n_sp, n_tp, heads, float(tok * n_sp)),
            out_shape=(
                pltpu.VMEM((rows_y, width), BF16),
                pltpu.VMEM((rows_w, cols), F32),
                pltpu.VMEM((2, cols), F32),
            ),
            in_specs=[any_spec] * 6 + [vmem_spec] * 2,
            out_specs=(vmem_spec,) * 3,
            scratch_shapes=[
                vm((tok, width), BF16),
                vm((width, cols), BF16), vm((width, cols), BF16), vm((width, cols), BF16), vm((width, cols), BF16),
                vm((tok, cols), BF16),
                vm((heads, 2, KDIM), F32), vm((n_sp, 2, KDIM), F32),
                *pieces,
                vm((2, n_chip, rows_w, cols), F32), vm((n_chip, rows_w, cols), F32),
                vm((n_chip, rows_w, cols), F32), vm((n_chip, rows_w, cols), F32),
                vm((4, n_tp, rows_y, quarter), F32), vm((4, rows_y, quarter), F32),
                vm((4, rows_y, quarter), F32), vm((8, rows_y, quarter), F32),
                vm((2 * heads, KDIM), F32), vm((n_sp, 2 * heads, KDIM), F32),
                pltpu.SemaphoreType.DMA((6,)),
                pltpu.SemaphoreType.DMA((10,)),
                pltpu.SemaphoreType.DMA((10,)),
                pltpu.SemaphoreType.DMA((12,)),
                pltpu.SemaphoreType.DMA((12,)),
            ],
            compiler_params=pltpu.CompilerParams(collective_id=0, has_side_effects=True),
        )(block_input, w_query, w_forget_fwd, w_forget_bwd, w_value, cotangent, floor_rate, gain.reshape(1, KDIM))

    return jax.shard_map(
        body,
        mesh=mesh,
        in_specs=(
            P("sp", None), P(None, "tp"), P(None, "tp"), P(None, "tp"), P(None, "tp"), P(None, "tp"), P(), P("sp", "tp"),
        ),
        out_specs=(P(("sp", "tp"), None), P("sp", "tp"), P(None, "tp")),
        check_vma=False,
    )
```

time: 49.4 us -> 46.3 us (0.937); the launches traced: 49.2 us -> 45.6 us
  Pallas kernels: 45.8 us -> 43.1 us
  local copies, waits for them, and re-layouts: 2.74 us -> 1.82 us
    pallas_call x1, Pallas kernels: 45.8 us -> 43.1 us  [body(): pl.pallas_call(functools.partial(kernel, n_sp, n_tp, heads, float(tok * n...]
    unnamed x7 -> x3, local copies, waits for them, and re-layouts: 2.74 us -> 1.82 us
where the time goes in v2:
time: 46.3 us; the launch traced here: 45.6 us
  Pallas kernels  43.1 us (93%)
  local copies, waits for them, and re-layouts  1.82 us (4%)
  between operations  0.64 us (1%)
    pallas_call x1, Pallas kernels, body(): pl.pallas_call(functools.partial(kernel, n_sp, n_tp, heads, float(tok * n...  43.1 us
    unnamed x3, local copies, waits for them, and re-layouts  1.82 us

profile of v2, /device:TPU:0, one launch (start us, length us, event | category | flops | bytes accessed | tf_op | source)
XLA Modules:
  0.0 45.6 jit_solution(15753815009926590811)
XLA Ops:
  0.6 43.1 %shard_map.103 = (bf16[32,1024]{1,0:T(8,128)(2,1)S(1)}, f32[32,256]{1,0:T(8,128)S(1)}, f32[2,256]{1,0:T(2,128)S(1)}) custom-call(bf16[128,1024]{1,0:T(8,128)(2,1)} %x_hbm.1, bf16[1024,256]{1,0:T(8,128)(2,1)} %wq_hbm.1, bf16[1024,256]{1,0:T(8,128)(2,1)} %wf_hbm.1, bf16[1024,256]{1,0:T(8,128)(2,1)} %wb_hbm.1, bf16[1024,256]{1,0:T(8,128)(2,1)} %wv_hbm.1, ...), custom_call_target="tpu_custom_call" | custom-call | tf_op jit(solution)/shard_map/pallas_call | solution.py:418
  43.7 0.6 %copy.14 = bf16[32,1024]{1,0:T(8,128)(2,1)} copy(bf16[32,1024]{1,0:T(8,128)(2,1)S(1)} %get-tuple-element.3) | data formatting | bytes 131072
  44.4 0.6 %copy.16 = f32[2,256]{1,0:T(2,128)} copy(f32[2,256]{1,0:T(2,128)S(1)} %get-tuple-element.5) | data formatting | bytes 4096
  45.0 0.6 %copy.15 = f32[32,256]{1,0:T(8,128)} copy(f32[32,256]{1,0:T(8,128)S(1)} %get-tuple-element.4) | data formatting | bytes 65536

commit v3 on v2

--- a/solution.py
+++ b/solution.py
@@ -53,7 +53,7 @@
     x_hbm, wq_hbm, wf_hbm, wb_hbm, wv_hbm, ct_hbm, rate_ref, gain_ref,
     gin_ref, gw_ref, gfl_ref,
     x_v, wq_v, wf_v, wb_v, wv_v, ct_v,
-    dec_s, dec_r, a1_s, a1_r, a2_s, a2_r, b1_s, b1_r, b2_s, b2_r,
+    a1_s, a1_r, a2_s, a2_r, b1_s, b1_r, b2_s, b2_r,
     w1_s, w1_r, w2_s, w2_r, y_s, rel_r, ysum_s, y_r, fl_s, fl_r,
     in_sem, snd, rcv, y_snd, y_rcv,
 ):
@@ -188,9 +188,9 @@
     dec_b = jnp.exp(cum_b[0:1])
     head = lambda a, h: a[:, h * KDIM : (h + 1) * KDIM]
     for h in range(heads):
-        dec_s[h, 0:1, :] = head(dec_f, h)
-        dec_s[h, 1:2, :] = head(dec_b, h)
-    dec_r[me] = dec_s[my_head]
+        for p in range(h * per, (h + 1) * per):
+            a1_s[p, 16:17, :] = head(dec_f, h)
+            a1_s[p, 17:18, :] = head(dec_b, h)
 
     grow_f, grow_b = jnp.exp(-cum_f), jnp.exp(-cum_b)
     kd_f, kd_b = key_f * grow_f, key_b * grow_b
@@ -206,7 +206,6 @@
     pl.semaphore_wait(barrier, n_sp + 1)
     for h in range(heads):
         to_owners(a1_s, a1_r, 1, h)
-    to_all(lambda to: dec_s.at[lax.div(to, per)], dec_r, 0)
 
     loaded(4)
     q = dot(x, wq_v[...], NN).astype(BF16).astype(F32) * q_scale
@@ -231,12 +230,11 @@
             result[j, up_rows, :] = up
             result[k, down_rows, :] = down
             if j < n_sp - 1:
-                up = up * dec_r[j, up_dir : up_dir + 1, :] + received[j, up_rows, :]
-                down = down * dec_r[k, down_dir : down_dir + 1, :] + received[k, down_rows, :]
+                up = up * a1_r[j, 16 + up_dir : 17 + up_dir, :] + received[j, up_rows, :]
+                down = down * a1_r[k, 16 + down_dir : 17 + down_dir, :] + received[k, down_rows, :]
 
     FWD, BWD = slice(0, 8), slice(8, 16)
 
-    arrived(0)
     arrived(1)
     owner_scan(a1_r, a2_s, FWD, 0, BWD, 1)
     give_back(a2_s, a2_r, 2)
@@ -412,7 +410,7 @@
         rows_y = tok // n_tp
         quarter = width // 4
         vm = pltpu.VMEM
-        pieces = [vm((n_sp, 16, KDIM), F32) for _ in range(8)]
+        pieces = [vm((n_sp, 18 if i < 2 else 16, KDIM), F32) for i in range(8)]
         any_spec = pl.BlockSpec(memory_space=pl.ANY)
         vmem_spec = pl.BlockSpec(memory_space=pltpu.VMEM)
         return pl.pallas_call(
@@ -428,7 +426,6 @@
                 vm((tok, width), BF16),
                 vm((width, cols), BF16), vm((width, cols), BF16), vm((width, cols), BF16), vm((width, cols), BF16),
                 vm((tok, cols), BF16),
-                vm((heads, 2, KDIM), F32), vm((n_sp, 2, KDIM), F32),
                 *pieces,
                 vm((2, n_chip, rows_w, cols), F32), vm((n_chip, rows_w, cols), F32),
                 vm((n_chip, rows_w, cols), F32), vm((n_chip, rows_w, cols), F32),

time: 46.3 us -> 45.1 us (0.974)
  Pallas kernels: 43.1 us -> 42 us
    pallas_call x1, Pallas kernels: 43.1 us -> 42 us  [body(): pl.pallas_call(functools.partial(kernel, n_sp, n_tp, heads, float(tok * n...]
where the time goes in v3:
time: 45.1 us; the launch traced here: 44.5 us
  Pallas kernels  42 us (93%)
  local copies, waits for them, and re-layouts  1.82 us (4%)
  between operations  0.64 us (1%)
    pallas_call x1, Pallas kernels, body(): pl.pallas_call(functools.partial(kernel, n_sp, n_tp, heads, float(tok * n...  42 us
    unnamed x3, local copies, waits for them, and re-layouts  1.82 us

profile of v3, /device:TPU:0, one launch (start us, length us, event | category | flops | bytes accessed | tf_op | source)
XLA Modules:
  0.0 44.5 jit_solution(1223206482844973664)
XLA Ops:
  0.6 42.0 %shard_map.103 = (bf16[32,1024]{1,0:T(8,128)(2,1)S(1)}, f32[32,256]{1,0:T(8,128)S(1)}, f32[2,256]{1,0:T(2,128)S(1)}) custom-call(bf16[128,1024]{1,0:T(8,128)(2,1)} %x_hbm.1, bf16[1024,256]{1,0:T(8,128)(2,1)} %wq_hbm.1, bf16[1024,256]{1,0:T(8,128)(2,1)} %wf_hbm.1, bf16[1024,256]{1,0:T(8,128)(2,1)} %wb_hbm.1, bf16[1024,256]{1,0:T(8,128)(2,1)} %wv_hbm.1, ...), custom_call_target="tpu_custom_call" | custom-call | tf_op jit(solution)/shard_map/pallas_call | solution.py:416
  42.7 0.6 %copy.14 = bf16[32,1024]{1,0:T(8,128)(2,1)} copy(bf16[32,1024]{1,0:T(8,128)(2,1)S(1)} %get-tuple-element.3) | data formatting | bytes 131072
  43.3 0.6 %copy.16 = f32[2,256]{1,0:T(2,128)} copy(f32[2,256]{1,0:T(2,128)S(1)} %get-tuple-element.5) | data formatting | bytes 4096
  43.9 0.6 %copy.15 = f32[32,256]{1,0:T(8,128)} copy(f32[32,256]{1,0:T(8,128)S(1)} %get-tuple-element.4) | data formatting | bytes 65536

commit v4 on v3

--- a/solution.py
+++ b/solution.py
@@ -287,9 +287,9 @@
     dk_f = [mm(d_low[h], q_fs[h], TN) for h in range(heads)]
     dk_b = [mm(d_high[h], q_bs[h], TN) for h in range(heads)]
     dv = [mm(scores[h], d_out[h], TN) for h in range(heads)]
-    quarter = width // 4
+    quarter = width // 2
     rows_y = tok // n_tp
-    for c in range(4):
+    for c in range(2):
         y_s[c] = dot(g_q, wq_v[c * quarter : (c + 1) * quarter, :], NT).reshape(n_tp, rows_y, quarter)
 
     arrived(4)
@@ -315,6 +315,20 @@
         d_rate = jnp.sum(d_key * sig_neg, axis=0, keepdims=True) * ((1.0 - opening) * (1.0 / seq_total))
         return d_raw.astype(BF16), d_rate
 
+    up, down, across = lax.rem(tp + 1, n_tp), lax.rem(tp + n_tp - 1, n_tp), lax.rem(tp + 2, n_tp)
+
+    def ring(src, dst, i, device):
+        return pltpu.make_async_remote_copy(
+            src_ref=src, dst_ref=dst, send_sem=y_snd.at[i], recv_sem=y_rcv.at[i],
+            device_id=device, device_id_type=MESH,
+        )
+
+    relay, direct, summed = [], [], []
+    for c in range(2):
+        ahead, behind = (right, left) if c % 2 == 0 else (left, right)
+        relay.append(ring(y_s.at[c, across], rel_r.at[c], c, ahead))
+        direct.append(ring(y_s.at[c, down if c % 2 == 0 else up], y_r.at[c], 2 + c, behind))
+        summed.append(ring(ysum_s.at[c], y_r.at[2 + c], 4 + c, ahead))
     for h in range(heads):
         head_arrived(b2_r, 5, h)
         back_f, back_b = state(b2_r, h, FWD), state(b2_r, h, BWD)
@@ -338,7 +352,7 @@
         fl_s[h : h + 1, :] = r_f
         fl_s[heads + h : heads + h + 1, :] = r_b
         mine = slice(h * KDIM, (h + 1) * KDIM)
-        for c in range(4):
+        for c in range(2):
             rows = slice(c * quarter, (c + 1) * quarter)
             y = (
                 dot(g_f, wf_v[rows, mine], NT)
@@ -346,30 +360,16 @@
                 + dot(g_v, wv_v[rows, mine], NT)
             )
             y_s[c] = y_s[c] + y.reshape(n_tp, rows_y, quarter)
-
-    up, down, across = lax.rem(tp + 1, n_tp), lax.rem(tp + n_tp - 1, n_tp), lax.rem(tp + 2, n_tp)
-
-    def ring(src, dst, i, device):
-        return pltpu.make_async_remote_copy(
-            src_ref=src, dst_ref=dst, send_sem=y_snd.at[i], recv_sem=y_rcv.at[i],
-            device_id=device, device_id_type=MESH,
-        )
-
-    relay, direct, summed = [], [], []
-    for c in range(4):
-        ahead, behind = (right, left) if c % 2 == 0 else (left, right)
-        relay.append(ring(y_s.at[c, across], rel_r.at[c], c, ahead))
-        direct.append(ring(y_s.at[c, down if c % 2 == 0 else up], y_r.at[c], 4 + c, behind))
-        summed.append(ring(ysum_s.at[c], y_r.at[4 + c], 8 + c, ahead))
-    for c in range(4):
-        relay[c].start()
-        begun(("relay", c), relay[c])
-    for c in range(4):
+            if h == heads - 1:
+                relay[c].start()
+                begun(("relay", c), relay[c])
+
+    to_all(lambda to: fl_s, fl_r, 9)
+    fl_r[me] = fl_s[...]
+    for c in range(2):
         direct[c].start()
         begun(("direct", c), direct[c])
-    to_all(lambda to: fl_s, fl_r, 9)
-    fl_r[me] = fl_s[...]
-    for c in range(4):
+    for c in range(2):
         arrived(("relay", c))
         ysum_s[c] = y_s[c, up if c % 2 == 0 else down] + rel_r[c]
         summed[c].start()
@@ -390,10 +390,10 @@
         acc = acc + w2_r[r]
     gw_ref[...] = acc * norm_scale
 
-    for c in range(4):
+    for c in range(2):
         arrived(("direct", c))
         arrived(("summed", c))
-        gin_ref[:, c * quarter : (c + 1) * quarter] = (y_s[c, tp] + y_r[c] + y_r[4 + c]).astype(BF16)
+        gin_ref[:, c * quarter : (c + 1) * quarter] = (y_s[c, tp] + y_r[c] + y_r[2 + c]).astype(BF16)
 
     drain()
 
@@ -408,7 +408,7 @@
         n_chip = n_sp // 2
         rows_w = width // n_sp
         rows_y = tok // n_tp
-        quarter = width // 4
+        quarter = width // 2
         vm = pltpu.VMEM
         pieces = [vm((n_sp, 18 if i < 2 else 16, KDIM), F32) for i in range(8)]
         any_spec = pl.BlockSpec(memory_space=pl.ANY)
@@ -429,7 +429,7 @@
                 *pieces,
                 vm((2, n_chip, rows_w, cols), F32), vm((n_chip, rows_w, cols), F32),
                 vm((n_chip, rows_w, cols), F32), vm((n_chip, rows_w, cols), F32),
-                vm((4, n_tp, rows_y, quarter), F32), vm((4, rows_y, quarter), F32),
+                vm((2, n_tp, rows_y, quarter), F32), vm((4, rows_y, quarter), F32),
                 vm((4, rows_y, quarter), F32), vm((8, rows_y, quarter), F32),
                 vm((2 * heads, KDIM), F32), vm((n_sp, 2 * heads, KDIM), F32),
                 pltpu.SemaphoreType.DMA((6,)),

time: 45.1 us -> 45 us (level)
  no operation moved by 1% of the time
where the time goes in v4:
time: 45 us; the launch traced here: 44.8 us
  Pallas kernels  42.3 us (94%)
  local copies, waits for them, and re-layouts  1.82 us (4%)
  between operations  0.64 us (1%)
    pallas_call x1, Pallas kernels, body(): pl.pallas_call(functools.partial(kernel, n_sp, n_tp, heads, float(tok * n...  42.3 us
    unnamed x3, local copies, waits for them, and re-layouts  1.82 us

profile of v4, /device:TPU:0, one launch (start us, length us, event | category | flops | bytes accessed | tf_op | source)
XLA Modules:
  0.0 44.8 jit_solution(15093580011152598578)
XLA Ops:
  0.6 42.3 %shard_map.103 = (bf16[32,1024]{1,0:T(8,128)(2,1)S(1)}, f32[32,256]{1,0:T(8,128)S(1)}, f32[2,256]{1,0:T(2,128)S(1)}) custom-call(bf16[128,1024]{1,0:T(8,128)(2,1)} %x_hbm.1, bf16[1024,256]{1,0:T(8,128)(2,1)} %wq_hbm.1, bf16[1024,256]{1,0:T(8,128)(2,1)} %wf_hbm.1, bf16[1024,256]{1,0:T(8,128)(2,1)} %wb_hbm.1, bf16[1024,256]{1,0:T(8,128)(2,1)} %wv_hbm.1, ...), custom_call_target="tpu_custom_call" | custom-call | tf_op jit(solution)/shard_map/pallas_call | solution.py:416
  43.0 0.6 %copy.14 = bf16[32,1024]{1,0:T(8,128)(2,1)} copy(bf16[32,1024]{1,0:T(8,128)(2,1)S(1)} %get-tuple-element.3) | data formatting | bytes 131072
  43.6 0.6 %copy.16 = f32[2,256]{1,0:T(2,128)} copy(f32[2,256]{1,0:T(2,128)S(1)} %get-tuple-element.5) | data formatting | bytes 4096
  44.2 0.6 %copy.15 = f32[32,256]{1,0:T(8,128)} copy(f32[32,256]{1,0:T(8,128)S(1)} %get-tuple-element.4) | data formatting | bytes 65536

commit v5 on v3

--- a/solution.py
+++ b/solution.py
@@ -364,11 +364,11 @@
     for c in range(4):
         relay[c].start()
         begun(("relay", c), relay[c])
+    to_all(lambda to: fl_s, fl_r, 9)
+    fl_r[me] = fl_s[...]
     for c in range(4):
         direct[c].start()
         begun(("direct", c), direct[c])
-    to_all(lambda to: fl_s, fl_r, 9)
-    fl_r[me] = fl_s[...]
     for c in range(4):
         arrived(("relay", c))
         ysum_s[c] = y_s[c, up if c % 2 == 0 else down] + rel_r[c]

time: 45.1 us -> 45.1 us (level)
  no operation moved by 1% of the time
where the time goes in v5:
time: 45.1 us; the launch traced here: 44.5 us
  Pallas kernels  42 us (93%)
  local copies, waits for them, and re-layouts  1.82 us (4%)
  between operations  0.64 us (1%)
    pallas_call x1, Pallas kernels, body(): pl.pallas_call(functools.partial(kernel, n_sp, n_tp, heads, float(tok * n...  42 us
    unnamed x3, local copies, waits for them, and re-layouts  1.82 us

profile of v5, /device:TPU:0, one launch (start us, length us, event | category | flops | bytes accessed | tf_op | source)
XLA Modules:
  0.0 44.5 jit_solution(14903957523057462342)
XLA Ops:
  0.6 42.0 %shard_map.103 = (bf16[32,1024]{1,0:T(8,128)(2,1)S(1)}, f32[32,256]{1,0:T(8,128)S(1)}, f32[2,256]{1,0:T(2,128)S(1)}) custom-call(bf16[128,1024]{1,0:T(8,128)(2,1)} %x_hbm.1, bf16[1024,256]{1,0:T(8,128)(2,1)} %wq_hbm.1, bf16[1024,256]{1,0:T(8,128)(2,1)} %wf_hbm.1, bf16[1024,256]{1,0:T(8,128)(2,1)} %wb_hbm.1, bf16[1024,256]{1,0:T(8,128)(2,1)} %wv_hbm.1, ...), custom_call_target="tpu_custom_call" | custom-call | tf_op jit(solution)/shard_map/pallas_call | solution.py:416
  42.7 0.6 %copy.14 = bf16[32,1024]{1,0:T(8,128)(2,1)} copy(bf16[32,1024]{1,0:T(8,128)(2,1)S(1)} %get-tuple-element.3) | data formatting | bytes 131072
  43.3 0.6 %copy.16 = f32[2,256]{1,0:T(2,128)} copy(f32[2,256]{1,0:T(2,128)S(1)} %get-tuple-element.5) | data formatting | bytes 4096
  43.9 0.6 %copy.15 = f32[32,256]{1,0:T(8,128)} copy(f32[32,256]{1,0:T(8,128)S(1)} %get-tuple-element.4) | data formatting | bytes 65536
